TPU v7x, 32 devices: a whole 2x2x4 slice. The times are simulated.
32 devices in a mesh: sp: 16 (over z, y, x), tp: 2 (over core).
Axes of the slice: x: 2, y: 2, z: 4, core: 2. Of those that a mesh axis runs over, the one named last changes fastest.
Arguments:
- tokens_in: bfloat16 [2048, 2048], P(('sp', 'tp')), may hold values from -9 to 9, as said below
- w_query: bfloat16 [2048, 2048], P(None, 'tp'), may hold values from -0.125 to 0.125
- w_key: bfloat16 [2048, 512], P(None, 'tp'), may hold values from -0.125 to 0.125
- w_value: bfloat16 [2048, 512], P(None, 'tp'), may hold values from -0.125 to 0.125
- w_out: bfloat16 [2048, 2048], P('tp'), may hold values from -0.125 to 0.125
- q_gain: float32 [64], replicated, may hold values from 0.1 to 14
- k_gain: float32 [64], replicated, may hold values from 0.1 to 14
Outputs:
- attended: bfloat16 [2048, 2048], P(('sp', 'tp'))
Inputs may be any that keep to these rules, and one draw needn't show every extreme that they name: `tokens_in`: activations whose mean differs from one block of 128 tokens to another.
All inputs are finite; a program needn't handle non-finite values.
Results may differ from a plain program's by a relative error of at most 0.014.
The roundings to bfloat16 on the way count: a program that leaves them out, or rounds other values in their place, can miss the bound.
Values may be sent and summed in bfloat16 or wider, within the bound.
A program may use at most 64 MiB of HBM per device.

v0:
```python
import functools

import jax
import jax.numpy as jnp
import numpy as np
from jax import lax
from jax.experimental import pallas as pl
from jax.experimental.pallas import tpu as pltpu
from jax.sharding import PartitionSpec as P

GRID_W = 64
LANES = 128
REACH = 1 << 20


def tables(token_count, head_dim):
    pairs = head_dim // 4
    lane = np.arange(LANES)
    freq = 10000.0 ** (-(lane % pairs) / pairs)
    sign = np.where(lane % (2 * pairs) < pairs, -1.0, 1.0)

    def both(count):
        angle = np.arange(count)[:, None] * freq[None, :]
        return np.concatenate([np.cos(angle), np.sin(angle) * sign], axis=1).astype(np.float32)

    return both(token_count // GRID_W), both(GRID_W)


def kernel(
    n_sp, n_tp, members, head_dim,
    tok_hbm, wq_hbm, wkv_hbms, wo_hbm, row_ref, col_ref, qg_ref, kg_ref, out_ref,
    x, wq, wkvs, wo, kv_out, kv_all, q_out, q_all, qm, k4, v1, peak, acc, m_out, m_all, o_acc, o_out, o_in,
    load_sem, x_send, x_recv, kv_send, kv_recv, line_send, on_send, q_send, q_recv, m_send, m_recv, o_send, o_recv,
):
    sp, tp = lax.axis_index("sp"), lax.axis_index("tp")
    own_rows = tok_hbm.shape[0]
    rows = own_rows * n_tp
    groups = n_sp // members
    plane, member = sp // members, sp % members
    query_cols = wq.shape[1]
    width = query_cols // members
    heads = width // head_dim
    first = plane * members

    def sp_copy(src, dst, send, recv, to):
        return pltpu.make_async_remote_copy(
            src_ref=src, dst_ref=dst, send_sem=send, recv_sem=recv,
            device_id={"sp": to}, device_id_type=pl.DeviceIdType.MESH)

    def tp_copy(src, dst, send, recv, to):
        return pltpu.make_async_remote_copy(
            src_ref=src, dst_ref=dst, send_sem=send, recv_sem=recv,
            device_id={"tp": to}, device_id_type=pl.DeviceIdType.MESH)

    def own_slice(index):
        return pl.ds(pl.multiple_of(index * own_rows, own_rows), own_rows)

    below, above = plane, groups - 1 - plane
    both_sides = jnp.minimum(below, above)

    def way(i):
        paired = i <= 2 * both_sides
        distance = jnp.where(paired, (i + 1) // 2, i - both_sides)
        upward = jnp.where(paired, i % 2, jnp.where(above > below, 1, 0))
        return distance, 2 * upward - 1

    def nearest(i):
        distance, side = way(i)
        return plane + distance * side

    loads = [pltpu.make_async_copy(tok_hbm, x.at[own_slice(tp)], load_sem.at[0])]
    for i, (src, dst) in enumerate(zip((*wkv_hbms, wq_hbm, wo_hbm), (*wkvs, wq, wo))):
        loads.append(pltpu.make_async_copy(src, dst, load_sem.at[i + 1]))
    for load in loads:
        load.start()
    barrier = pltpu.get_barrier_semaphore()
    for step in range(1, n_tp):
        pl.semaphore_signal(barrier, inc=1, device_id={"tp": (tp + step) % n_tp}, device_id_type=pl.DeviceIdType.MESH)

    for step in range(1, members):
        pl.semaphore_signal(barrier, inc=1, device_id={"sp": first + (member + step) % members},
                            device_id_type=pl.DeviceIdType.MESH)

    def greet(i, carry):
        @pl.when(way(i)[0] <= REACH)
        def _():
            pl.semaphore_signal(barrier, inc=1, device_id={"sp": nearest(i) * members + member},
                                device_id_type=pl.DeviceIdType.MESH)
        return carry

    lax.fori_loop(1, groups, greet, 0)

    lane = lax.broadcasted_iota(jnp.int32, (rows, LANES), 1)
    low = lane % head_dim < head_dim // 2
    left = lane % (head_dim // 2) < head_dim // 4
    even = lane < head_dim
    cos_parts, sin_parts = [], []
    per_dev = rows // GRID_W
    low_g = low[:GRID_W]
    for i in range(per_dev):
        line = row_ref[pl.ds(sp * per_dev + i, 1), :]
        cos_parts.append(jnp.where(low_g, jnp.broadcast_to(line[:, :LANES], (GRID_W, LANES)), col_ref[:, :LANES]))
        sin_parts.append(jnp.where(low_g, jnp.broadcast_to(line[:, LANES:], (GRID_W, LANES)), col_ref[:, LANES:]))
    cosine = jnp.concatenate(cos_parts, axis=0)
    sine = jnp.concatenate(sin_parts, axis=0)
    ones_r = lax.broadcasted_iota(jnp.int32, (LANES, LANES), 0) // head_dim
    ones_c = lax.broadcasted_iota(jnp.int32, (LANES, LANES), 1) // head_dim
    block = jnp.where(ones_r == ones_c, 1.0, 0.0).astype(jnp.bfloat16)
    gain_q = jnp.concatenate([qg_ref[...]] * (LANES // head_dim), axis=1) * head_dim ** (-0.5)
    gain_k = jnp.concatenate([kg_ref[...]] * (LANES // head_dim), axis=1)

    def turned(u, gain):
        square = u * u
        high = square.astype(jnp.bfloat16)
        rest = (square - high.astype(jnp.float32)).astype(jnp.bfloat16)
        total = jnp.dot(high, block, preferred_element_type=jnp.float32) + jnp.dot(
            rest, block, preferred_element_type=jnp.float32)
        n = u * lax.rsqrt(total * (1.0 / head_dim) + 1e-06) * gain
        quarter = head_dim // 4
        other = jnp.where(left, pltpu.roll(n, LANES - quarter, 1), pltpu.roll(n, quarter, 1))
        return n * cosine + other * sine

    def project(w):
        return jnp.dot(x[...], w, preferred_element_type=jnp.float32).astype(jnp.bfloat16).astype(jnp.float32)

    peak[...] = jnp.full_like(peak, -1e30)
    acc[...] = jnp.zeros_like(acc)

    loads[0].wait()
    pl.semaphore_wait(
        barrier, jnp.minimum(below, REACH) + jnp.minimum(above, REACH) + members - 1 + n_tp - 1)
    x_copies = []
    for step in range(1, n_tp):
        mine = x.at[own_slice(tp)]
        copy = tp_copy(mine, mine, x_send.at[step], x_recv.at[step], (tp + step) % n_tp)
        copy.start()
        x_copies.append(copy)
    for step in range(1, n_tp):
        theirs = x.at[own_slice((tp + n_tp - step) % n_tp)]
        tp_copy(theirs, theirs, x_send.at[step], x_recv.at[step], (tp + step) % n_tp).wait_recv()

    for i in range(len(wkvs)):
        loads[1 + i].wait()
    if len(wkvs) == 2:
        keys = project(wkvs[0][...])
        vals = project(wkvs[1][...])
        for pair in range(members // 2):
            cut = slice(pair * LANES, (pair + 1) * LANES)
            k, v = turned(keys[:, cut], gain_k), vals[:, cut]
            kv_out[2 * pair] = jnp.where(even, k, pltpu.roll(v, head_dim, 1)).astype(jnp.bfloat16)
            kv_out[2 * pair + 1] = jnp.where(even, pltpu.roll(k, head_dim, 1), v).astype(jnp.bfloat16)
    else:
        both = project(wkvs[0][...])
        kv_out[0] = jnp.where(even, turned(both, gain_k), both).astype(jnp.bfloat16)

    kv_all[sp] = kv_out[member]

    def kv_copy(step):
        to = (member + step) % members
        return sp_copy(kv_out.at[to], kv_all.at[sp], kv_send.at[step], kv_recv.at[sp], first + to)

    for step in range(1, members):
        kv_copy(step).start()

    def line_copy(i, c):
        slot = kv_all.at[first + c]
        return sp_copy(slot, slot, line_send.at[i * members + c], kv_recv.at[first + c], nearest(i) * members + member)

    def onward(i, act):
        distance, side = way(i)

        @pl.when((distance >= REACH) & (plane - side >= 0) & (plane - side < groups))
        def _():
            for c in range(members):
                slot = (plane + distance * side) * members + c
                act(sp_copy(kv_all.at[slot], kv_all.at[slot], on_send.at[i * members + c], kv_recv.at[slot],
                            (plane - side) * members + member))

    def along(step):
        def one(i, carry):
            @pl.when(way(i)[0] <= REACH)
            def _():
                line_copy(i, (member + step) % members).start()
            return carry

        lax.fori_loop(1, groups, one, 0)

    along(0)

    def wait_kv(slot):
        sp_copy(kv_all.at[slot], kv_all.at[slot], kv_send.at[0], kv_recv.at[slot], sp).wait_recv()

    loads[1 + len(wkvs)].wait()
    for p in range(members):
        u = project(wq[:, p * width:(p + 1) * width])
        for t in range(width // LANES):
            cut = slice(t * LANES, (t + 1) * LANES)
            q_out[p, :, cut] = turned(u[:, cut], gain_q).astype(jnp.bfloat16)

    def q_copy(step):
        to = (member + step) % members
        return sp_copy(q_out.at[to], q_all.at[member], q_send.at[step], q_recv.at[member], first + to)

    for step in range(1, members):
        q_copy(step).start()
    q_all[member] = q_out[member]

    for step in range(1, members):
        wait_kv(first + (member + members - step) % members)
        along(members - step)

    wide_lane = lax.broadcasted_iota(jnp.int32, (rows, width), 1) // head_dim

    def mask_queries(c):
        q = q_all[c]
        for g in range(heads):
            qm[pl.ds(pl.multiple_of((c * heads + g) * rows, rows), rows), :] = jnp.where(
                wide_lane == g, q, jnp.zeros_like(q))

    tall = heads * rows

    def prepare(slot, c):
        tile = kv_all[slot].astype(jnp.float32)
        turned_tile = pltpu.roll(tile, head_dim, 1)
        kk = jnp.where(even, tile, turned_tile).astype(jnp.bfloat16)
        place = pl.ds(c * rows, rows)
        for t in range(width // LANES):
            k4[place, t * LANES:(t + 1) * LANES] = kk
        v1[place, :] = jnp.where(even, turned_tile, 1.0).astype(jnp.bfloat16)

    def attend(c):
        place = pl.ds(pl.multiple_of(c * tall, tall), tall)
        scores = lax.dot_general(qm[place, :], k4[...], (((1,), (1,)), ((), ())),
                                 preferred_element_type=jnp.float32)
        before = peak[place, :]
        now = jnp.maximum(before, jnp.max(scores, axis=1, keepdims=True))
        expo = jnp.exp(scores - jnp.concatenate([now] * (scores.shape[1] // LANES), axis=1))
        peak[place, :] = now
        acc[place, :] = acc[place, :] * jnp.exp(before - now) + jnp.dot(
            expo.astype(jnp.bfloat16), v1[...], preferred_element_type=jnp.float32)

    def finish(c):
        parts = []
        for pair in range(heads // 2):
            halves = []
            for g in (2 * pair, 2 * pair + 1):
                piece = acc[pl.ds(pl.multiple_of((c * heads + g) * rows, rows), rows), :]
                halves.append(piece / pltpu.roll(piece, head_dim, 1))
            parts.append(jnp.where(even, halves[0], pltpu.roll(halves[1], head_dim, 1)))
        m_out[c] = jnp.concatenate(parts, axis=1).astype(jnp.bfloat16)

    def m_copy(step):
        to = (member + step) % members
        return sp_copy(m_out.at[to], m_all.at[member], m_send.at[step], m_recv.at[member], first + to)

    for c in range(members):
        prepare(first + c, c)
    for step in range(members):
        c = (member + members - step) % members
        if step:
            sp_copy(q_out.at[c], q_all.at[c], q_send.at[step], q_recv.at[c], first + c).wait_recv()
        mask_queries(c)
        attend(c)

    def fetch(i):
        base = nearest(i) * members
        for c in range(members):
            wait_kv(base + c)
        onward(i, lambda copy: copy.start())
        for c in range(members):
            prepare(base + c, c)

    def whole_group(i, carry):
        fetch(i)
        for c in range(members):
            attend(c)
        return carry

    lax.fori_loop(1, groups - 1, whole_group, 0)
    fetch(groups - 1)
    for step in range(1, members + 1):
        c = (member + step) % members
        attend(c)
        finish(c)
        if step < members:
            m_copy(step).start()
    m_all[member] = m_out[member]

    loads[2 + len(wkvs)].wait()
    for step in range(members):
        s = (member + members - step) % members
        if step:
            sp_copy(m_out.at[s], m_all.at[s], m_send.at[step], m_recv.at[s], first + s).wait_recv()
        term = jnp.dot(m_all[s], wo[pl.ds(pl.multiple_of(s * width, width), width), :],
                       preferred_element_type=jnp.float32)
        if step == 0:
            o_acc[...] = term
        else:
            o_acc[...] += term
    o_copies = []
    for step in range(1, n_tp):
        to = (tp + step) % n_tp
        o_out[step] = o_acc[own_slice(to), :].astype(jnp.bfloat16)
        copy = tp_copy(o_out.at[step], o_in.at[step], o_send.at[step], o_recv.at[step], to)
        copy.start()
        o_copies.append(copy)
    result = o_acc[own_slice(tp), :].astype(jnp.bfloat16).astype(jnp.float32)
    for step in range(1, n_tp):
        o_copies[step - 1].wait_recv()
        result = result + o_in[step].astype(jnp.float32)
    out_ref[...] = result.astype(jnp.bfloat16)

    for copy in x_copies + o_copies:
        copy.wait_send()
    for step in range(1, members):
        kv_copy(step).wait_send()
        q_copy(step).wait_send()
        m_copy(step).wait_send()

    def sent_along(i, carry):
        @pl.when(way(i)[0] <= REACH)
        def _():
            for c in range(members):
                line_copy(i, c).wait_send()

        onward(i, lambda copy: copy.wait_send())
        return carry

    lax.fori_loop(1, groups, sent_along, 0)


def solution(mesh):
    n_sp, n_tp = mesh.shape["sp"], mesh.shape["tp"]

    def body(tokens_in, w_query, w_key, w_value, w_out, q_gain, k_gain):
        head_dim = q_gain.shape[0]
        own_rows, depth = tokens_in.shape
        rows = own_rows * n_tp
        query_cols, key_cols = w_query.shape[1], w_key.shape[1]
        members = key_cols // head_dim
        width = query_cols // members
        heads = width // head_dim
        if key_cols % LANES:
            wkv = (jnp.concatenate([w_key, w_value], axis=1),)
        else:
            wkv = (w_key, w_value)
        row_table, col_table = tables(rows * n_sp, head_dim)
        bf, f32 = jnp.bfloat16, jnp.float32
        hbm = pl.BlockSpec(memory_space=pltpu.HBM)
        vmem = pl.BlockSpec(memory_space=pltpu.VMEM)
        dma = pltpu.SemaphoreType.DMA
        call = pl.pallas_call(
            functools.partial(kernel, n_sp, n_tp, members, head_dim),
            out_shape=jax.ShapeDtypeStruct((own_rows, w_out.shape[1]), bf),
            in_specs=[hbm, hbm, (hbm,) * len(wkv), hbm, vmem, vmem, vmem, vmem],
            out_specs=vmem,
            scratch_shapes=[
                pltpu.VMEM((rows, depth), bf),
                pltpu.VMEM(w_query.shape, bf),
                tuple(pltpu.VMEM(w.shape, bf) for w in wkv),
                pltpu.VMEM(w_out.shape, bf),
                pltpu.VMEM((members, rows, LANES), bf),
                pltpu.VMEM((n_sp, rows, LANES), bf),
                pltpu.VMEM((members, rows, width), bf),
                pltpu.VMEM((members, rows, width), bf),
                pltpu.VMEM((members * heads * rows, width), bf),
                pltpu.VMEM((members * rows, width), bf),
                pltpu.VMEM((members * rows, LANES), bf),
                pltpu.VMEM((members * heads * rows, LANES), f32),
                pltpu.VMEM((members * heads * rows, LANES), f32),
                pltpu.VMEM((members, rows, width), bf),
                pltpu.VMEM((members, rows, width), bf),
                pltpu.VMEM((rows, w_out.shape[1]), f32),
                pltpu.VMEM((n_tp, own_rows, w_out.shape[1]), bf),
                pltpu.VMEM((n_tp, own_rows, w_out.shape[1]), bf),
                dma((6,)),
                dma((n_tp,)), dma((n_tp,)),
                dma((members,)), dma((n_sp,)), dma((n_sp,)), dma((n_sp,)),
                dma((members,)), dma((members,)),
                dma((members,)), dma((members,)),
                dma((n_tp,)), dma((n_tp,)),
            ],
            compiler_params=pltpu.CompilerParams(
                collective_id=0, has_side_effects=True, vmem_limit_bytes=56 * 1024 * 1024),
        )
        return call(tokens_in, w_query, wkv, w_out, jnp.asarray(row_table), jnp.asarray(col_table),
                    q_gain.reshape(1, head_dim), k_gain.reshape(1, head_dim))

    return jax.shard_map(
        body,
        mesh=mesh,
        in_specs=(
            P(("sp", "tp"), None),
            P(None, "tp"),
            P(None, "tp"),
            P(None, "tp"),
            P("tp", None),
            P(),
            P(),
        ),
        out_specs=P(("sp", "tp"), None),
        check_vma=False,
    )
```

profile of v0, /device:TPU:0, one launch (start us, length us, event | category | flops | bytes accessed | tf_op | source)
XLA Modules:
  0.0 34.0 jit_solution(5752604101866483028)
XLA Ops:
  0.0 32.3 %shard_map.91 = bf16[64,2048]{1,0:T(8,128)(2,1)} custom-call(bf16[64,2048]{1,0:T(8,128)(2,1)} %tok_hbm.1, bf16[2048,1024]{1,0:T(8,128)(2,1)} %wq_hbm.1, bf16[2048,256]{1,0:T(8,128)(2,1)} %wkv_hbms_0_.1, bf16[2048,256]{1,0:T(8,128)(2,1)} %wkv_hbms_1_.1, bf16[1024,2048]{1,0:T(8,128)(2,1)} %wo_hbm.1, f32[32,256]{1,0:T(8,128)} %constant.4.clone.row_ref, ...), custom_call_target="tpu_custom_call" | custom-call | tf_op jit(solution)/shard_map/pallas_call | solution.py:386
  32.3 1.7 %copy.11 = bf16[64,2048]{1,0:T(8,128)(2,1)} copy(bf16[64,2048]{1,0:T(8,128)(2,1)} %shard_map.91) | data formatting | bytes 524288
where the time goes:
time: 34.2 us; the launch traced here: 34 us
  Pallas kernels  32.3 us (94%)
  local copies, waits for them, and re-layouts  1.67 us (5%)
    pallas_call x1, Pallas kernels, body(): call(tokens_in, w_query, wkv, w_out, jnp.asarray(row_table), jnp.asarray(...  32.3 us
    unnamed x1, local copies, waits for them, and re-layouts  1.67 us

commit v1 on v0

v1 whole, which is shorter than its diff:
```python
import functools

import jax
import jax.numpy as jnp
import numpy as np
from jax import lax
from jax.experimental import pallas as pl
from jax.experimental.pallas import tpu as pltpu
from jax.sharding import PartitionSpec as P

GRID_W = 64
LANES = 128
ONES = 16
X_CUTS = 4
O_CUTS = 4
STRAIGHT = (1, 2)


def tables(token_count, head_dim):
    pairs = head_dim // 4
    lane = np.arange(LANES)
    freq = 10000.0 ** (-(lane % pairs) / pairs)
    sign = np.where(lane % (2 * pairs) < pairs, -1.0, 1.0)

    def both(count):
        angle = np.arange(count)[:, None] * freq[None, :]
        return np.concatenate([np.cos(angle), np.sin(angle) * sign], axis=1).astype(np.float32)

    return both(token_count // GRID_W), both(GRID_W)


def kernel(
    n_sp, n_tp, members, head_dim,
    tok_hbm, wq_hbm, wkv_hbms, wo_hbm, row_hbm, col_hbm, qg_hbm, kg_hbm, out_ref,
    x, wq, wkvs, wo, row_ref, col_ref, qg_ref, kg_ref,
    kv_out, kv_all, q_out, q_all, qs, vt, sc, pb, acc, peak, m_out, m_all, o_acc, o_out, o_in,
    load_sem, x_send, x_recv, kv_send, kv_recv, up_send, down_send, cross_send, on_send,
    q_send, q_recv, m_send, m_recv, o_send, o_recv,
):
    bf, f32 = jnp.bfloat16, jnp.float32
    sp, tp = lax.axis_index("sp"), lax.axis_index("tp")
    own_rows, depth = tok_hbm.shape
    rows = own_rows * n_tp
    groups = n_sp // members
    plane, member = sp // members, sp % members
    width = wq.shape[1] // members
    heads = width // head_dim
    tall = heads * rows
    keys = members * rows
    first = plane * members
    below, above = plane, groups - 1 - plane
    both_sides = jnp.minimum(below, above)

    def peer(step):
        other, bit = member, 1
        while bit <= step:
            if step & bit:
                other = other + bit - 2 * bit * ((member // bit) % 2)
            bit *= 2
        return other

    def sp_copy(src, dst, send, recv, to):
        return pltpu.make_async_remote_copy(
            src_ref=src, dst_ref=dst, send_sem=send, recv_sem=recv,
            device_id={"sp": to}, device_id_type=pl.DeviceIdType.MESH)

    def tp_copy(src, dst, send, recv, to):
        return pltpu.make_async_remote_copy(
            src_ref=src, dst_ref=dst, send_sem=send, recv_sem=recv,
            device_id={"tp": to}, device_id_type=pl.DeviceIdType.MESH)

    def own_slice(index):
        return pl.ds(pl.multiple_of(index * own_rows, own_rows), own_rows)

    def way(i):
        paired = i <= 2 * both_sides
        distance = jnp.where(paired, (i + 1) // 2, i - both_sides)
        upward = jnp.where(paired, i % 2, jnp.where(above > below, 1, 0))
        return distance, 2 * upward - 1

    barrier = pltpu.get_barrier_semaphore()
    for step in range(1, n_tp):
        pl.semaphore_signal(barrier, inc=1, device_id={"tp": (tp + step) % n_tp}, device_id_type=pl.DeviceIdType.MESH)
    for step in range(1, members):
        pl.semaphore_signal(barrier, inc=1, device_id={"sp": first + peer(step)}, device_id_type=pl.DeviceIdType.MESH)

    def greet(when, to):
        @pl.when(when)
        def _():
            pl.semaphore_signal(barrier, inc=1, device_id={"sp": to}, device_id_type=pl.DeviceIdType.MESH)

    crossing = [step for step in STRAIGHT if step < members]
    greet(below > 0, sp - members)
    greet(above > 0, sp + members)
    greet((below > 1) & (above > 0), sp - 2 * members)
    greet((above > 1) & (below > 0), sp + 2 * members)
    for step in crossing:
        greet((plane < 2) & (above > 0), (plane + 1) * members + peer(step))
        greet((plane > 0) & (above > 1), (plane + 2) * members + peer(step))

    def count(fact):
        return jnp.where(fact, 1, 0)

    targets = (n_tp - 1 + members - 1 + count(below > 0) + count(above > 0) + count(below > 2) + count(above > 2)
               + len(crossing) * count(below > 0))

    small = 1 + len(wkvs)
    pairs_of = [(tok_hbm, x.at[own_slice(tp)]), *zip(wkv_hbms, wkvs), (row_hbm, row_ref), (col_hbm, col_ref),
                (qg_hbm, qg_ref), (kg_hbm, kg_ref), (wq_hbm, wq), (wo_hbm, wo)]
    loads = [pltpu.make_async_copy(src, dst, load_sem.at[i]) for i, (src, dst) in enumerate(pairs_of)]
    for load in loads[:small + 4]:
        load.start()

    lane = lax.broadcasted_iota(jnp.int32, (rows, LANES), 1)
    low = lane % head_dim < head_dim // 2
    left = lane % (head_dim // 2) < head_dim // 4
    even = lane < head_dim
    ones_r = lax.broadcasted_iota(jnp.int32, (LANES, LANES), 0) // head_dim
    ones_c = lax.broadcasted_iota(jnp.int32, (LANES, LANES), 1) // head_dim
    block = jnp.where(ones_r == ones_c, 1.0, 0.0).astype(bf)
    vt[:ONES, :] = jnp.ones((ONES, 2 * keys), bf)

    pl.semaphore_wait(barrier, targets)
    cut_depth = depth // X_CUTS

    def x_copy(step, j):
        cols = pl.ds(j * cut_depth, cut_depth)
        return tp_copy(tok_hbm.at[:, cols], x.at[own_slice(tp), cols], x_send.at[step, j], x_recv.at[step, j],
                       (tp + step) % n_tp)

    for j in range(X_CUTS):
        for step in range(1, n_tp):
            x_copy(step, j).start()
    for load in loads[small + 4:]:
        load.start()

    for load in loads[small:small + 4]:
        load.wait()
    cos_parts, sin_parts = [], []
    per_dev = rows // GRID_W
    low_g = low[:GRID_W]
    for i in range(per_dev):
        line = row_ref[pl.ds(sp * per_dev + i, 1), :]
        cos_parts.append(jnp.where(low_g, jnp.broadcast_to(line[:, :LANES], (GRID_W, LANES)), col_ref[:, :LANES]))
        sin_parts.append(jnp.where(low_g, jnp.broadcast_to(line[:, LANES:], (GRID_W, LANES)), col_ref[:, LANES:]))
    cosine = jnp.concatenate(cos_parts, axis=0)
    sine = jnp.concatenate(sin_parts, axis=0)
    gain_q = jnp.concatenate([qg_ref[...]] * (LANES // head_dim), axis=1) * head_dim ** (-0.5)
    gain_k = jnp.concatenate([kg_ref[...]] * (LANES // head_dim), axis=1)

    def turned(u, gain):
        square = u * u
        high = square.astype(bf)
        rest = (square - high.astype(f32)).astype(bf)
        total = jnp.dot(high, block, preferred_element_type=f32) + jnp.dot(
            rest, block, preferred_element_type=f32)
        n = u * lax.rsqrt(total * (1.0 / head_dim) + 1e-06) * gain
        quarter = head_dim // 4
        other = jnp.where(left, pltpu.roll(n, LANES - quarter, 1), pltpu.roll(n, quarter, 1))
        return n * cosine + other * sine

    for load in loads[:small]:
        load.wait()
    sums = [None] * len(wkvs)
    for j in range(X_CUTS):
        cols = slice(j * cut_depth, (j + 1) * cut_depth)
        for step in range(1, n_tp):
            theirs = x.at[own_slice((tp + n_tp - step) % n_tp), pl.ds(j * cut_depth, cut_depth)]
            tp_copy(theirs, theirs, x_send.at[step, j], x_recv.at[step, j], (tp + step) % n_tp).wait_recv()
        for i in range(len(wkvs)):
            part = jnp.dot(x[:, cols], wkvs[i][cols, :], preferred_element_type=f32)
            sums[i] = part if j == 0 else sums[i] + part
    sums = [s.astype(bf).astype(f32) for s in sums]
    if len(wkvs) == 2:
        for pair in range(members // 2):
            cut = slice(pair * LANES, (pair + 1) * LANES)
            k, v = turned(sums[0][:, cut], gain_k), sums[1][:, cut]
            kv_out[2 * pair] = jnp.where(even, k, pltpu.roll(v, head_dim, 1)).astype(bf)
            kv_out[2 * pair + 1] = jnp.where(even, pltpu.roll(k, head_dim, 1), v).astype(bf)
    else:
        kv_out[0] = jnp.where(even, turned(sums[0], gain_k), sums[0]).astype(bf)

    def kv_copy(step):
        return sp_copy(kv_out.at[peer(step)], kv_all.at[sp], kv_send.at[step], kv_recv.at[sp], first + peer(step))

    def line(src, slot, send, to_plane):
        return sp_copy(src, kv_all.at[slot], send, kv_recv.at[slot], to_plane * members + member)

    def both_ways(src, slot, step, act):
        if step in crossing:
            beside, beyond = below > 2, below < 0
        else:
            beside, beyond = below > 0, below > 2

        @pl.when(beside)
        def _():
            act(line(src, slot, down_send.at[0, step], plane - 1))

        @pl.when(above > 0)
        def _():
            act(line(src, slot, up_send.at[0, step], plane + 1))

        @pl.when(beyond)
        def _():
            act(line(src, slot, down_send.at[1, step], plane - 2))

        @pl.when(above > 2)
        def _():
            act(line(src, slot, up_send.at[1, step], plane + 2))

    def straight(step, act):
        to_plane = jnp.where(plane > 2, plane - 2, plane - 1)

        @pl.when(plane > 0)
        def _():
            act(sp_copy(kv_out.at[peer(step)], kv_all.at[sp], cross_send.at[step], kv_recv.at[sp],
                        to_plane * members + peer(step)))

    def start(copy):
        copy.start()

    def wait_send(copy):
        copy.wait_send()

    def wait_kv(slot):
        sp_copy(kv_all.at[slot], kv_all.at[slot], kv_send.at[0], kv_recv.at[slot], sp).wait_recv()

    both_ways(kv_out.at[member], sp, 0, start)
    for step in range(1, members):
        kv_copy(step).start()
    for step in crossing:
        straight(step, start)
    kv_all[sp] = kv_out[member]

    loads[small + 4].wait()

    def q_copy(step):
        return sp_copy(q_out.at[step], q_all.at[step], q_send.at[step], q_recv.at[step], first + peer(step))

    def spread(step, q):
        for g in range(heads):
            u = q[:, (g // 2) * LANES:(g // 2 + 1) * LANES].astype(f32)
            u = u if g % 2 == 0 else pltpu.roll(u, head_dim, 1)
            qs[(step * heads + g) * rows:(step * heads + g + 1) * rows, :] = jnp.where(even, u, 0.0).astype(bf)

    def plane_relay(step):
        slot = first + peer(step)
        wait_kv(slot)
        both_ways(kv_all.at[slot], slot, step, start)

    def raw_queries(step):
        part = wq[:, pl.ds(pl.multiple_of(peer(step) * width, width), width)]
        return jnp.dot(x[...], part, preferred_element_type=f32)

    order = (*range(members - 1, 0, -1), 0)
    raw = raw_queries(order[0])
    for n, step in enumerate(order):
        u = raw.astype(bf).astype(f32)
        if n + 1 < members:
            raw = raw_queries(order[n + 1])
        for t in range(width // LANES):
            cut = slice(t * LANES, (t + 1) * LANES)
            q_out[step, :, cut] = turned(u[:, cut], gain_q).astype(bf)
    near_first = tuple(range(members))
    far_first = (*range(members - 1, 0, -1), 0)

    def onward(i):
        distance, side = way(i)
        target = plane - side
        inside = (target > 0) & (target < groups - 1)
        needed = (target >= 0) & (target < groups) & ((distance > 1) | jnp.logical_not(inside))
        return (plane + distance * side) * members, target, needed

    def relay(i, steps):
        base, to_plane, needed = onward(i)

        @pl.when(needed)
        def _():
            for step in steps:
                slot = base + peer(step)
                wait_kv(slot)
                line(kv_all.at[slot], slot, on_send.at[slot], to_plane).start()

    at_end = (below == 0) | (above == 0)

    def send_queries():
        for step in far_first[:-1]:
            q_copy(step).start()

    @pl.when(at_end)
    def _():
        send_queries()

    if groups > 1:
        relay(1, (0,))
    if groups > 3:
        relay(3, (0,))
    for step in near_first[1:]:
        plane_relay(step)
    @pl.when(jnp.logical_not(at_end))
    def _():
        send_queries()

    if groups > 1 and members > 1:
        relay(1, near_first[1:3])
    if groups > 2:
        relay(2, near_first)
    if groups > 3 and members > 1:
        relay(3, near_first[1:3])

    def prepare(slots):
        for c, slot in enumerate(slots):
            flipped = kv_all[slot].astype(f32).T
            vt[ONES:, c * rows:(c + 1) * rows] = flipped[head_dim:].astype(bf)

    def score(slots, step, bank):
        k = jnp.concatenate([kv_all[slot] for slot in slots], axis=0)
        sc[bank, :len(slots) * rows] = lax.dot_general(
            k, qs[step * tall:(step + 1) * tall, :], (((1,), (1,)), ((), ())), preferred_element_type=f32)

    def weigh(count, step, bank, fresh):
        place = slice(step * tall, (step + 1) * tall)
        s = sc[bank, :count]
        top = jnp.max(jnp.max(s.reshape(count // 8, 8, tall), axis=0), axis=0, keepdims=True)
        now = jnp.broadcast_to(top, (8, tall))
        fade = None
        if not fresh:
            before = peak[:, place]
            now = jnp.maximum(before, now)
            fade = jnp.exp(before - now)
        peak[:, place] = now
        pb[bank, :count] = jnp.exp(s - jnp.broadcast_to(now[:1], (count, tall))).astype(bf)
        return fade

    def gather(count, step, bank, fade):
        place = slice(step * tall, (step + 1) * tall)
        new = jnp.dot(vt[:, :count], pb[bank, :count], preferred_element_type=f32)
        if fade is not None:
            new = acc[:, place] * jnp.broadcast_to(fade[:1], (ONES + head_dim, tall)) + new
        acc[:, place] = new

    def sweep(slots, steps, fresh=False, done=None):
        count = len(slots) * rows
        prepare(slots)
        score(slots, steps[0], 0)
        fades = [None] * len(steps)
        for n, step in enumerate(steps):
            if n + 1 < len(steps):
                score(slots, steps[n + 1], (n + 1) % 2)
            fades[n] = weigh(count, step, n % 2, fresh)
            if n:
                gather(count, steps[n - 1], (n - 1) % 2, fades[n - 1])
                if done:
                    done(steps[n - 1])
        gather(count, steps[-1], (len(steps) - 1) % 2, fades[-1])
        if done:
            done(steps[-1])

    def m_copy(step):
        return sp_copy(m_out.at[step], m_all.at[step], m_send.at[step], m_recv.at[step], first + peer(step))

    def finish(step):
        for pair in range(heads // 2):
            halves = []
            for g in (2 * pair, 2 * pair + 1):
                piece = acc[:, (step * heads + g) * rows:(step * heads + g + 1) * rows]
                halves.append(piece[ONES:] * jnp.concatenate([1.0 / piece[:8]] * (head_dim // 8), axis=0))
            mixed = jnp.concatenate(halves, axis=0).T.astype(bf)
            (m_out if step else m_all)[step, :, pair * LANES:(pair + 1) * LANES] = mixed
        if step:
            m_copy(step).start()

    def slots_of(i):
        base, _, needed = onward(i)
        return [base + peer(step) for step in near_first], needed

    def fetch(slots, needed):
        @pl.when(jnp.logical_not(needed))
        def _():
            for slot in slots:
                wait_kv(slot)

    own = [sp if step == 0 else first + peer(step) for step in near_first]
    spread(0, q_out[0])
    sweep(own, (0,), fresh=True)
    if groups > 1 and members > 1:
        relay(1, near_first[3:])
        if groups > 3:
            relay(3, near_first[3:])
    for step in range(1, members):
        sp_copy(q_out.at[step], q_all.at[step], q_send.at[step], q_recv.at[step], first + peer(step)).wait_recv()
        spread(step, q_all[step])
    if members > 1:
        sweep(own, tuple(range(1, members)), fresh=True)

    def whole_group(i, carry):
        slots, needed = slots_of(i)
        fetch(slots, needed)
        sweep(slots, near_first)
        if groups > 4:
            @pl.when(i + 3 < groups)
            def _():
                relay(i + 3, near_first)
        return carry

    if groups > 1:
        joined = max(1, groups - 2)
        lax.fori_loop(1, joined, whole_group, 0)
        last_slots = []
        for i in range(joined, groups):
            slots, needed = slots_of(i)
            fetch(slots, needed)
            last_slots += slots
        sweep(last_slots, far_first, done=finish)
    else:
        for step in far_first:
            finish(step)

    loads[small + 5].wait()
    cut_out = wo.shape[1] // O_CUTS

    def o_copy(step, j):
        cols = pl.ds(j * cut_out, cut_out)
        return tp_copy(o_out.at[step, :, cols], o_in.at[step, :, cols], o_send.at[step, j], o_recv.at[step, j],
                       (tp + step) % n_tp)

    def mixed_share(step, j):
        share = pl.ds(pl.multiple_of(peer(step) * width, width), width)
        return jnp.dot(m_all[step], wo[share, j * cut_out:(j + 1) * cut_out], preferred_element_type=f32)

    for step in (0, *far_first[:-1]):
        if step:
            sp_copy(m_out.at[step], m_all.at[step], m_send.at[step], m_recv.at[step], first + peer(step)).wait_recv()
        term = mixed_share(step, 0)
        for j in range(O_CUTS):
            cols = slice(j * cut_out, (j + 1) * cut_out)
            total = o_acc[:, cols] + term if step else term
            if j + 1 < O_CUTS:
                term = mixed_share(step, j + 1)
            o_acc[:, cols] = total
            if step == min(1, members - 1):
                for other in range(1, n_tp):
                    o_out[other, :, cols] = o_acc[own_slice((tp + other) % n_tp), cols].astype(bf)
                    o_copy(other, j).start()
    for j in range(O_CUTS):
        cols = slice(j * cut_out, (j + 1) * cut_out)
        result = o_acc[own_slice(tp), cols].astype(bf).astype(f32)
        for other in range(1, n_tp):
            o_copy(other, j).wait_recv()
            result = result + o_in[other, :, cols].astype(f32)
        out_ref[:, cols] = result.astype(bf)

    for j in range(X_CUTS):
        for step in range(1, n_tp):
            x_copy(step, j).wait_send()
    for j in range(O_CUTS):
        for step in range(1, n_tp):
            o_copy(step, j).wait_send()
    both_ways(kv_out.at[member], sp, 0, wait_send)
    for step in range(1, members):
        kv_copy(step).wait_send()
        q_copy(step).wait_send()
        m_copy(step).wait_send()
        both_ways(kv_all.at[first + peer(step)], first + peer(step), step, wait_send)
        if step in crossing:
            straight(step, wait_send)

    def sent(i, carry):
        base, to_plane, needed = onward(i)

        @pl.when(needed)
        def _():
            for step in near_first:
                slot = base + peer(step)
                line(kv_all.at[slot], slot, on_send.at[slot], to_plane).wait_send()

        return carry

    lax.fori_loop(1, groups, sent, 0)


def solution(mesh):
    n_sp, n_tp = mesh.shape["sp"], mesh.shape["tp"]

    def body(tokens_in, w_query, w_key, w_value, w_out, q_gain, k_gain):
        head_dim = q_gain.shape[0]
        own_rows, depth = tokens_in.shape
        rows = own_rows * n_tp
        query_cols, key_cols = w_query.shape[1], w_key.shape[1]
        members = key_cols // head_dim
        width = query_cols // members
        heads = width // head_dim
        if key_cols % LANES:
            wkv = (jnp.concatenate([w_key, w_value], axis=1),)
        else:
            wkv = (w_key, w_value)
        row_table, col_table = tables(rows * n_sp, head_dim)
        bf, f32 = jnp.bfloat16, jnp.float32
        hbm = pl.BlockSpec(memory_space=pltpu.HBM)
        vmem = pl.BlockSpec(memory_space=pltpu.VMEM)
        dma = pltpu.SemaphoreType.DMA
        out_cols = w_out.shape[1]
        call = pl.pallas_call(
            functools.partial(kernel, n_sp, n_tp, members, head_dim),
            out_shape=pltpu.VMEM((own_rows, out_cols), bf),
            in_specs=[hbm, hbm, (hbm,) * len(wkv), hbm, hbm, hbm, hbm, hbm],
            out_specs=vmem,
            scratch_shapes=[
                pltpu.VMEM((rows, depth), bf),
                pltpu.VMEM(w_query.shape, bf),
                tuple(pltpu.VMEM(w.shape, bf) for w in wkv),
                pltpu.VMEM(w_out.shape, bf),
                pltpu.VMEM(row_table.shape, f32),
                pltpu.VMEM(col_table.shape, f32),
                pltpu.VMEM((1, head_dim), f32),
                pltpu.VMEM((1, head_dim), f32),
                pltpu.VMEM((members, rows, LANES), bf),
                pltpu.VMEM((n_sp, rows, LANES), bf),
                pltpu.VMEM((members, rows, width), bf),
                pltpu.VMEM((members, rows, width), bf),
                pltpu.VMEM((members * heads * rows, LANES), bf),
                pltpu.VMEM((ONES + head_dim, 2 * members * rows), bf),
                pltpu.VMEM((2, 2 * members * rows, heads * rows), f32),
                pltpu.VMEM((2, 2 * members * rows, heads * rows), bf),
                pltpu.VMEM((ONES + head_dim, members * heads * rows), f32),
                pltpu.VMEM((8, members * heads * rows), f32),
                pltpu.VMEM((members, rows, width), bf),
                pltpu.VMEM((members, rows, width), bf),
                pltpu.VMEM((rows, out_cols), f32),
                pltpu.VMEM((n_tp, own_rows, out_cols), bf),
                pltpu.VMEM((n_tp, own_rows, out_cols), bf),
                dma((9,)),
                dma((n_tp, X_CUTS)), dma((n_tp, X_CUTS)),
                dma((members,)), dma((n_sp,)), dma((2, members)), dma((2, members)), dma((members,)), dma((n_sp,)),
                dma((members,)), dma((members,)),
                dma((members,)), dma((members,)),
                dma((n_tp, O_CUTS)), dma((n_tp, O_CUTS)),
            ],
            compiler_params=pltpu.CompilerParams(
                collective_id=0, has_side_effects=True, vmem_limit_bytes=56 * 1024 * 1024),
        )
        return call(tokens_in, w_query, wkv, w_out, jnp.asarray(row_table), jnp.asarray(col_table),
                    q_gain.reshape(1, head_dim), k_gain.reshape(1, head_dim))

    return jax.shard_map(
        body,
        mesh=mesh,
        in_specs=(
            P(("sp", "tp"), None),
            P(None, "tp"),
            P(None, "tp"),
            P(None, "tp"),
            P("tp", None),
            P(),
            P(),
        ),
        out_specs=P(("sp", "tp"), None),
        check_vma=False,
    )
```

time: 34.2 us -> 30 us (0.88)
  Pallas kernels: 32.3 us -> 29.1 us
  local copies, waits for them, and re-layouts: 1.67 us -> 0.71 us
    pallas_call x1, Pallas kernels: 32.3 us -> 29.1 us  [body(): call(tokens_in, w_query, wkv, w_out, jnp.asarray(row_table), jnp.asarray(...]
    unnamed x1, local copies, waits for them, and re-layouts: 1.67 us -> 0.71 us
where the time goes in v1:
time: 30 us; the launch traced here: 29.8 us
  Pallas kernels  29.1 us (97%)
  local copies, waits for them, and re-layouts  0.71 us (2%)
    pallas_call x1, Pallas kernels, body(): call(tokens_in, w_query, wkv, w_out, jnp.asarray(row_table), jnp.asarray(...  29.1 us
    unnamed x1, local copies, waits for them, and re-layouts  0.71 us

profile of v1, /device:TPU:0, one launch (start us, length us, event | category | flops | bytes accessed | tf_op | source)
XLA Modules:
  0.0 29.8 jit_solution(15446165448991931256)
XLA Ops:
  0.0 29.1 %shard_map.91 = bf16[64,2048]{1,0:T(8,128)(2,1)S(1)} custom-call(bf16[64,2048]{1,0:T(8,128)(2,1)} %tok_hbm.1, bf16[2048,1024]{1,0:T(8,128)(2,1)} %wq_hbm.1, bf16[2048,256]{1,0:T(8,128)(2,1)} %wkv_hbms_0_.1, bf16[2048,256]{1,0:T(8,128)(2,1)} %wkv_hbms_1_.1, bf16[1024,2048]{1,0:T(8,128)(2,1)} %wo_hbm.1, f32[32,256]{1,0:T(8,128)} %constant.4.clone.row_hbm, ...), custom_call_target="tpu_custom_call" | custom-call | tf_op jit(solution)/shard_map/pallas_call | solution.py:542
  29.1 0.7 %copy.11 = bf16[64,2048]{1,0:T(8,128)(2,1)} copy(bf16[64,2048]{1,0:T(8,128)(2,1)S(1)} %shard_map.91) | data formatting | bytes 524288

commit v2 on v1

--- a/solution.py
+++ b/solution.py
@@ -11,9 +11,10 @@
 GRID_W = 64
 LANES = 128
 ONES = 16
-X_CUTS = 4
-O_CUTS = 4
+X_CUTS = 1
+O_CUTS = 2
 STRAIGHT = (1, 2)
+LATE_BESIDE = False
 
 
 def tables(token_count, head_dim):
@@ -34,8 +35,7 @@
     tok_hbm, wq_hbm, wkv_hbms, wo_hbm, row_hbm, col_hbm, qg_hbm, kg_hbm, out_ref,
     x, wq, wkvs, wo, row_ref, col_ref, qg_ref, kg_ref,
     kv_out, kv_all, q_out, q_all, qs, vt, sc, pb, acc, peak, m_out, m_all, o_acc, o_out, o_in,
-    load_sem, x_send, x_recv, kv_send, kv_recv, up_send, down_send, cross_send, on_send,
-    q_send, q_recv, m_send, m_recv, o_send, o_recv,
+    load_sem, x_send, x_recv, kv_recv, own_send, on_send, q_recv, m_recv, o_recv,
 ):
     bf, f32 = jnp.bfloat16, jnp.float32
     sp, tp = lax.axis_index("sp"), lax.axis_index("tp")
@@ -49,6 +49,7 @@
     keys = members * rows
     first = plane * members
     below, above = plane, groups - 1 - plane
+    peers = max(1, members - 1)
     both_sides = jnp.minimum(below, above)
 
     def peer(step):
@@ -96,19 +97,21 @@
     greet((above > 1) & (below > 0), sp + 2 * members)
     for step in crossing:
         greet((plane < 2) & (above > 0), (plane + 1) * members + peer(step))
-        greet((plane > 0) & (above > 1), (plane + 2) * members + peer(step))
+        greet((plane > 1) & (above > 1), (plane + 2) * members + peer(step))
+        greet((plane == 0) & (above > 2), (plane + 3) * members + peer(step))
+    greet((plane == 0) & (above > 2), sp + 3 * members)
 
     def count(fact):
         return jnp.where(fact, 1, 0)
 
-    targets = (n_tp - 1 + members - 1 + count(below > 0) + count(above > 0) + count(below > 2) + count(above > 2)
+    targets = (n_tp - 1 + members - 1 + count(below > 0) + count(above > 0) + count(below > 2) + count(above > 2) + count(below == 3)
                + len(crossing) * count(below > 0))
 
     small = 1 + len(wkvs)
     pairs_of = [(tok_hbm, x.at[own_slice(tp)]), *zip(wkv_hbms, wkvs), (row_hbm, row_ref), (col_hbm, col_ref),
                 (qg_hbm, qg_ref), (kg_hbm, kg_ref), (wq_hbm, wq), (wo_hbm, wo)]
-    loads = [pltpu.make_async_copy(src, dst, load_sem.at[i]) for i, (src, dst) in enumerate(pairs_of)]
-    for load in loads[:small + 4]:
+    loads = [pltpu.make_async_copy(src, dst, load_sem.at[(i + 1) % len(pairs_of)]) for i, (src, dst) in enumerate(pairs_of)]
+    for load in loads:
         load.start()
 
     lane = lax.broadcasted_iota(jnp.int32, (rows, LANES), 1)
@@ -118,22 +121,20 @@
     ones_r = lax.broadcasted_iota(jnp.int32, (LANES, LANES), 0) // head_dim
     ones_c = lax.broadcasted_iota(jnp.int32, (LANES, LANES), 1) // head_dim
     block = jnp.where(ones_r == ones_c, 1.0, 0.0).astype(bf)
-    vt[:ONES, :] = jnp.ones((ONES, 2 * keys), bf)
-
+    vt[:ONES, :] = jnp.ones((ONES, 3 * keys), bf)
+
+    loads[0].wait()
     pl.semaphore_wait(barrier, targets)
     cut_depth = depth // X_CUTS
 
     def x_copy(step, j):
         cols = pl.ds(j * cut_depth, cut_depth)
-        return tp_copy(tok_hbm.at[:, cols], x.at[own_slice(tp), cols], x_send.at[step, j], x_recv.at[step, j],
+        return tp_copy(x.at[own_slice(tp), cols], x.at[own_slice(tp), cols], x_send.at[step - 1, j], x_recv.at[step - 1, j],
                        (tp + step) % n_tp)
 
     for j in range(X_CUTS):
         for step in range(1, n_tp):
             x_copy(step, j).start()
-    for load in loads[small + 4:]:
-        load.start()
-
     for load in loads[small:small + 4]:
         load.wait()
     cos_parts, sin_parts = [], []
@@ -159,14 +160,14 @@
         other = jnp.where(left, pltpu.roll(n, LANES - quarter, 1), pltpu.roll(n, quarter, 1))
         return n * cosine + other * sine
 
-    for load in loads[:small]:
+    for load in loads[1:small]:
         load.wait()
     sums = [None] * len(wkvs)
     for j in range(X_CUTS):
         cols = slice(j * cut_depth, (j + 1) * cut_depth)
         for step in range(1, n_tp):
             theirs = x.at[own_slice((tp + n_tp - step) % n_tp), pl.ds(j * cut_depth, cut_depth)]
-            tp_copy(theirs, theirs, x_send.at[step, j], x_recv.at[step, j], (tp + step) % n_tp).wait_recv()
+            tp_copy(theirs, theirs, x_send.at[step - 1, j], x_recv.at[step - 1, j], (tp + step) % n_tp).wait_recv()
         for i in range(len(wkvs)):
             part = jnp.dot(x[:, cols], wkvs[i][cols, :], preferred_element_type=f32)
             sums[i] = part if j == 0 else sums[i] + part
@@ -181,39 +182,51 @@
         kv_out[0] = jnp.where(even, turned(sums[0], gain_k), sums[0]).astype(bf)
 
     def kv_copy(step):
-        return sp_copy(kv_out.at[peer(step)], kv_all.at[sp], kv_send.at[step], kv_recv.at[sp], first + peer(step))
+        return sp_copy(kv_out.at[peer(step)], kv_all.at[sp], load_sem.at[step], kv_recv.at[sp], first + peer(step))
 
     def line(src, slot, send, to_plane):
         return sp_copy(src, kv_all.at[slot], send, kv_recv.at[slot], to_plane * members + member)
 
-    def both_ways(src, slot, step, act):
+    def both_ways(src, slot, step, act, late=False):
         if step in crossing:
-            beside, beyond = below > 2, below < 0
+            far, beside, beyond = below < 0, below > 2, below == 3
         else:
-            beside, beyond = below > 0, below > 2
-
-        @pl.when(beside)
-        def _():
-            act(line(src, slot, down_send.at[0, step], plane - 1))
+            far, beside, beyond = below == 3, below > 0, below > 2
+        if late:
+            @pl.when(below == 3)
+            def _():
+                if LATE_BESIDE:
+                    act(line(src, slot, own_send.at[0, step], plane - 1))
+                act(line(src, slot, own_send.at[own_send.shape[0] - 1 if groups > 4 else 1, step], plane - 2))
+
+            return
+
+        @pl.when(far)
+        def _():
+            act(line(src, slot, own_send.at[2, step], plane - 3))
+
+        @pl.when(beside & (below != 3) if LATE_BESIDE else beside)
+        def _():
+            act(line(src, slot, own_send.at[0, step], plane - 1))
 
         @pl.when(above > 0)
         def _():
-            act(line(src, slot, up_send.at[0, step], plane + 1))
-
-        @pl.when(beyond)
-        def _():
-            act(line(src, slot, down_send.at[1, step], plane - 2))
+            act(line(src, slot, own_send.at[1, step], plane + 1))
+
+        @pl.when(beyond & (below != 3))
+        def _():
+            act(line(src, slot, own_send.at[own_send.shape[0] - 1 if groups > 4 else 1, step], plane - 2))
 
         @pl.when(above > 2)
         def _():
-            act(line(src, slot, up_send.at[1, step], plane + 2))
+            act(line(src, slot, own_send.at[2, step], plane + 2))
 
     def straight(step, act):
-        to_plane = jnp.where(plane > 2, plane - 2, plane - 1)
+        to_plane = jnp.where(plane > 3, plane - 2, jnp.where(plane == 3, plane - 3, plane - 1))
 
         @pl.when(plane > 0)
         def _():
-            act(sp_copy(kv_out.at[peer(step)], kv_all.at[sp], cross_send.at[step], kv_recv.at[sp],
+            act(sp_copy(kv_out.at[peer(step)], kv_all.at[sp], own_send.at[jnp.where(plane > 3, own_send.shape[0] - 1, jnp.where(plane == 3, 2, 0)), step], kv_recv.at[sp],
                         to_plane * members + peer(step)))
 
     def start(copy):
@@ -223,7 +236,7 @@
         copy.wait_send()
 
     def wait_kv(slot):
-        sp_copy(kv_all.at[slot], kv_all.at[slot], kv_send.at[0], kv_recv.at[slot], sp).wait_recv()
+        sp_copy(kv_all.at[slot], kv_all.at[slot], load_sem.at[1], kv_recv.at[slot], sp).wait_recv()
 
     both_ways(kv_out.at[member], sp, 0, start)
     for step in range(1, members):
@@ -235,7 +248,7 @@
     loads[small + 4].wait()
 
     def q_copy(step):
-        return sp_copy(q_out.at[step], q_all.at[step], q_send.at[step], q_recv.at[step], first + peer(step))
+        return sp_copy(q_out.at[step], q_all.at[step], load_sem.at[peers + step], q_recv.at[step - 1], first + peer(step))
 
     def spread(step, q):
         for g in range(heads):
@@ -268,7 +281,8 @@
         distance, side = way(i)
         target = plane - side
         inside = (target > 0) & (target < groups - 1)
-        needed = (target >= 0) & (target < groups) & ((distance > 1) | jnp.logical_not(inside))
+        beyond = (distance > 1) & jnp.logical_not((distance == 2) & (target == 0) & (side > 0))
+        needed = (target >= 0) & (target < groups) & (beyond | ((distance == 1) & jnp.logical_not(inside)))
         return (plane + distance * side) * members, target, needed
 
     def relay(i, steps):
@@ -279,7 +293,7 @@
             for step in steps:
                 slot = base + peer(step)
                 wait_kv(slot)
-                line(kv_all.at[slot], slot, on_send.at[slot], to_plane).start()
+                line(kv_all.at[slot], slot, on_send.at[i if groups > 4 else i % 2, step], to_plane).start()
 
     at_end = (below == 0) | (above == 0)
 
@@ -301,17 +315,21 @@
     def _():
         send_queries()
 
+    def late_ways(act):
+        both_ways(kv_out.at[member], sp, 0, act, late=True)
+        for step in near_first[1:]:
+            both_ways(kv_all.at[first + peer(step)], first + peer(step), step, act, late=True)
+
+    late_ways(start)
     if groups > 1 and members > 1:
-        relay(1, near_first[1:3])
+        relay(1, near_first[1:])
     if groups > 2:
-        relay(2, near_first)
-    if groups > 3 and members > 1:
-        relay(3, near_first[1:3])
-
-    def prepare(slots):
+        relay(2, (0,))
+
+    def prepare(slots, offset):
         for c, slot in enumerate(slots):
             flipped = kv_all[slot].astype(f32).T
-            vt[ONES:, c * rows:(c + 1) * rows] = flipped[head_dim:].astype(bf)
+            vt[ONES:, offset + c * rows:offset + (c + 1) * rows] = flipped[head_dim:].astype(bf)
 
     def score(slots, step, bank):
         k = jnp.concatenate([kv_all[slot] for slot in slots], axis=0)
@@ -332,32 +350,29 @@
         pb[bank, :count] = jnp.exp(s - jnp.broadcast_to(now[:1], (count, tall))).astype(bf)
         return fade
 
-    def gather(count, step, bank, fade):
+    def gather(offset, count, step, bank, fade):
         place = slice(step * tall, (step + 1) * tall)
-        new = jnp.dot(vt[:, :count], pb[bank, :count], preferred_element_type=f32)
+        new = jnp.dot(vt[:, offset:offset + count], pb[bank, :count], preferred_element_type=f32)
         if fade is not None:
             new = acc[:, place] * jnp.broadcast_to(fade[:1], (ONES + head_dim, tall)) + new
         acc[:, place] = new
 
-    def sweep(slots, steps, fresh=False, done=None):
-        count = len(slots) * rows
-        prepare(slots)
-        score(slots, steps[0], 0)
-        fades = [None] * len(steps)
-        for n, step in enumerate(steps):
-            if n + 1 < len(steps):
-                score(slots, steps[n + 1], (n + 1) % 2)
-            fades[n] = weigh(count, step, n % 2, fresh)
+    def run(tasks, fresh=False):
+        score(tasks[0][0], tasks[0][2], 0)
+        fades = []
+        for n in range(len(tasks) + 1):
+            if n + 1 < len(tasks):
+                score(tasks[n + 1][0], tasks[n + 1][2], (n + 1) % 2)
+            if n < len(tasks):
+                fades.append(weigh(len(tasks[n][0]) * rows, tasks[n][2], n % 2, fresh))
             if n:
-                gather(count, steps[n - 1], (n - 1) % 2, fades[n - 1])
-                if done:
-                    done(steps[n - 1])
-        gather(count, steps[-1], (len(steps) - 1) % 2, fades[-1])
-        if done:
-            done(steps[-1])
+                slots, offset, step, last = tasks[n - 1]
+                gather(offset, len(slots) * rows, step, (n - 1) % 2, fades[n - 1])
+                if last:
+                    finish(step)
 
     def m_copy(step):
-        return sp_copy(m_out.at[step], m_all.at[step], m_send.at[step], m_recv.at[step], first + peer(step))
+        return sp_copy(m_out.at[step], m_all.at[step], load_sem.at[peers + step], m_recv.at[step - 1], first + peer(step))
 
     def finish(step):
         for pair in range(heads // 2):
@@ -382,21 +397,26 @@
 
     own = [sp if step == 0 else first + peer(step) for step in near_first]
     spread(0, q_out[0])
-    sweep(own, (0,), fresh=True)
-    if groups > 1 and members > 1:
-        relay(1, near_first[3:])
-        if groups > 3:
-            relay(3, near_first[3:])
+    prepare(own, 0)
+    run([(own, 0, 0, False)], fresh=True)
+    if groups > 2 and members > 1:
+        relay(2, near_first[1:])
+    if groups > 3 and members > 1:
+        relay(3, near_first[1:])
     for step in range(1, members):
-        sp_copy(q_out.at[step], q_all.at[step], q_send.at[step], q_recv.at[step], first + peer(step)).wait_recv()
+        sp_copy(q_out.at[step], q_all.at[step], load_sem.at[peers + step], q_recv.at[step - 1], first + peer(step)).wait_recv()
         spread(step, q_all[step])
     if members > 1:
-        sweep(own, tuple(range(1, members)), fresh=True)
+        run([(own, 0, step, False) for step in near_first[1:]], fresh=True)
+
+    deferred = groups == 4 and members > 1
+    spare = 2 * keys
 
     def whole_group(i, carry):
         slots, needed = slots_of(i)
         fetch(slots, needed)
-        sweep(slots, near_first)
+        prepare(slots, spare)
+        run([(slots, spare, step, False) for step in near_first[1 if deferred else 0:]])
         if groups > 4:
             @pl.when(i + 3 < groups)
             def _():
@@ -405,14 +425,25 @@
 
     if groups > 1:
         joined = max(1, groups - 2)
-        lax.fori_loop(1, joined, whole_group, 0)
+        if deferred:
+            whole_group(1, 0)
+        else:
+            lax.fori_loop(1, joined, whole_group, 0)
         last_slots = []
         for i in range(joined, groups):
             slots, needed = slots_of(i)
             fetch(slots, needed)
+            prepare(slots, len(last_slots) * rows)
             last_slots += slots
-        sweep(last_slots, far_first, done=finish)
+        tasks = [(last_slots, 0, step, True) for step in far_first]
+        if deferred:
+            tasks.insert(-1, (slots_of(1)[0], spare, 0, False))
+        for step in near_first[1:]:
+            q_copy(step).wait_send()
+        run(tasks)
     else:
+        for step in near_first[1:]:
+            q_copy(step).wait_send()
         for step in far_first:
             finish(step)
 
@@ -421,7 +452,7 @@
 
     def o_copy(step, j):
         cols = pl.ds(j * cut_out, cut_out)
-        return tp_copy(o_out.at[step, :, cols], o_in.at[step, :, cols], o_send.at[step, j], o_recv.at[step, j],
+        return tp_copy(o_out.at[step, :, cols], o_in.at[step, :, cols], load_sem.at[1 + 2 * peers + (step - 1) * O_CUTS + j], o_recv.at[step - 1, j],
                        (tp + step) % n_tp)
 
     def mixed_share(step, j):
@@ -430,7 +461,7 @@
 
     for step in (0, *far_first[:-1]):
         if step:
-            sp_copy(m_out.at[step], m_all.at[step], m_send.at[step], m_recv.at[step], first + peer(step)).wait_recv()
+            sp_copy(m_out.at[step], m_all.at[step], load_sem.at[peers + step], m_recv.at[step - 1], first + peer(step)).wait_recv()
         term = mixed_share(step, 0)
         for j in range(O_CUTS):
             cols = slice(j * cut_out, (j + 1) * cut_out)
@@ -457,9 +488,9 @@
         for step in range(1, n_tp):
             o_copy(step, j).wait_send()
     both_ways(kv_out.at[member], sp, 0, wait_send)
+    late_ways(wait_send)
     for step in range(1, members):
         kv_copy(step).wait_send()
-        q_copy(step).wait_send()
         m_copy(step).wait_send()
         both_ways(kv_all.at[first + peer(step)], first + peer(step), step, wait_send)
         if step in crossing:
@@ -472,7 +503,7 @@
         def _():
             for step in near_first:
                 slot = base + peer(step)
-                line(kv_all.at[slot], slot, on_send.at[slot], to_plane).wait_send()
+                line(kv_all.at[slot], slot, on_send.at[i if groups > 4 else i % 2, step], to_plane).wait_send()
 
         return carry
 
@@ -500,6 +531,7 @@
         vmem = pl.BlockSpec(memory_space=pltpu.VMEM)
         dma = pltpu.SemaphoreType.DMA
         out_cols = w_out.shape[1]
+        groups, peers = n_sp // members, max(1, members - 1)
         call = pl.pallas_call(
             functools.partial(kernel, n_sp, n_tp, members, head_dim),
             out_shape=pltpu.VMEM((own_rows, out_cols), bf),
@@ -519,7 +551,7 @@
                 pltpu.VMEM((members, rows, width), bf),
                 pltpu.VMEM((members, rows, width), bf),
                 pltpu.VMEM((members * heads * rows, LANES), bf),
-                pltpu.VMEM((ONES + head_dim, 2 * members * rows), bf),
+                pltpu.VMEM((ONES + head_dim, 3 * members * rows), bf),
                 pltpu.VMEM((2, 2 * members * rows, heads * rows), f32),
                 pltpu.VMEM((2, 2 * members * rows, heads * rows), bf),
                 pltpu.VMEM((ONES + head_dim, members * heads * rows), f32),
@@ -529,12 +561,12 @@
                 pltpu.VMEM((rows, out_cols), f32),
                 pltpu.VMEM((n_tp, own_rows, out_cols), bf),
                 pltpu.VMEM((n_tp, own_rows, out_cols), bf),
-                dma((9,)),
-                dma((n_tp, X_CUTS)), dma((n_tp, X_CUTS)),
-                dma((members,)), dma((n_sp,)), dma((2, members)), dma((2, members)), dma((members,)), dma((n_sp,)),
-                dma((members,)), dma((members,)),
-                dma((members,)), dma((members,)),
-                dma((n_tp, O_CUTS)), dma((n_tp, O_CUTS)),
+                dma((max(7 + len(wkv), 1 + 2 * peers + (n_tp - 1) * O_CUTS),)),
+                dma((n_tp - 1, X_CUTS)), dma((n_tp - 1, X_CUTS)),
+                dma((n_sp,)), dma((3 if groups <= 4 else 4, members)),
+                dma((2 if groups <= 4 else groups, members)),
+                dma((peers,)), dma((peers,)),
+                dma((n_tp - 1, O_CUTS)),
             ],
             compiler_params=pltpu.CompilerParams(
                 collective_id=0, has_side_effects=True, vmem_limit_bytes=56 * 1024 * 1024),

time: 30 us -> 28 us (0.933)
  Pallas kernels: 29.1 us -> 27.1 us
    pallas_call x1, Pallas kernels: 29.1 us -> 27.1 us  [body(): call(tokens_in, w_query, wkv, w_out, jnp.asarray(row_table), jnp.asarray(...]
where the time goes in v2:
time: 28 us; the launch traced here: 27.8 us
  Pallas kernels  27.1 us (97%)
  local copies, waits for them, and re-layouts  0.71 us (3%)
    pallas_call x1, Pallas kernels, body(): call(tokens_in, w_query, wkv, w_out, jnp.asarray(row_table), jnp.asarray(...  27.1 us
    unnamed x1, local copies, waits for them, and re-layouts  0.71 us

profile of v2, /device:TPU:0, one launch (start us, length us, event | category | flops | bytes accessed | tf_op | source)
XLA Modules:
  0.0 27.8 jit_solution(2738992223626143278)
XLA Ops:
  0.0 27.1 %shard_map.91 = bf16[64,2048]{1,0:T(8,128)(2,1)S(1)} custom-call(bf16[64,2048]{1,0:T(8,128)(2,1)} %tok_hbm.1, bf16[2048,1024]{1,0:T(8,128)(2,1)} %wq_hbm.1, bf16[2048,256]{1,0:T(8,128)(2,1)} %wkv_hbms_0_.1, bf16[2048,256]{1,0:T(8,128)(2,1)} %wkv_hbms_1_.1, bf16[1024,2048]{1,0:T(8,128)(2,1)} %wo_hbm.1, f32[32,256]{1,0:T(8,128)} %constant.4.clone.row_hbm, ...), custom_call_target="tpu_custom_call" | custom-call | tf_op jit(solution)/shard_map/pallas_call | solution.py:574
  27.1 0.7 %copy.11 = bf16[64,2048]{1,0:T(8,128)(2,1)} copy(bf16[64,2048]{1,0:T(8,128)(2,1)S(1)} %shard_map.91) | data formatting | bytes 524288

commit v3 on v2

--- a/solution.py
+++ b/solution.py
@@ -14,6 +14,7 @@
 X_CUTS = 1
 O_CUTS = 2
 STRAIGHT = (1, 2)
+HALVES = False
 LATE_BESIDE = False
 
 
@@ -331,59 +332,69 @@
             flipped = kv_all[slot].astype(f32).T
             vt[ONES:, offset + c * rows:offset + (c + 1) * rows] = flipped[head_dim:].astype(bf)
 
-    def score(slots, step, bank):
+    pairs = heads // 2
+    half = 2 * rows
+
+    def score(slots, place, bank):
         k = jnp.concatenate([kv_all[slot] for slot in slots], axis=0)
-        sc[bank, :len(slots) * rows] = lax.dot_general(
-            k, qs[step * tall:(step + 1) * tall, :], (((1,), (1,)), ((), ())), preferred_element_type=f32)
-
-    def weigh(count, step, bank, fresh):
-        place = slice(step * tall, (step + 1) * tall)
-        s = sc[bank, :count]
-        top = jnp.max(jnp.max(s.reshape(count // 8, 8, tall), axis=0), axis=0, keepdims=True)
-        now = jnp.broadcast_to(top, (8, tall))
+        sc[bank, :len(slots) * rows, :place.stop - place.start] = lax.dot_general(
+            k, qs[place, :], (((1,), (1,)), ((), ())), preferred_element_type=f32)
+
+    def weigh(count, place, bank, fresh):
+        size = place.stop - place.start
+        s = sc[bank, :count, :size]
+        top = jnp.max(jnp.max(s.reshape(count // 8, 8, size), axis=0), axis=0, keepdims=True)
+        now = jnp.broadcast_to(top, (8, size))
         fade = None
         if not fresh:
             before = peak[:, place]
             now = jnp.maximum(before, now)
             fade = jnp.exp(before - now)
         peak[:, place] = now
-        pb[bank, :count] = jnp.exp(s - jnp.broadcast_to(now[:1], (count, tall))).astype(bf)
+        pb[bank, :count, :size] = jnp.exp(s - jnp.broadcast_to(now[:1], (count, size))).astype(bf)
         return fade
 
-    def gather(offset, count, step, bank, fade):
-        place = slice(step * tall, (step + 1) * tall)
-        new = jnp.dot(vt[:, offset:offset + count], pb[bank, :count], preferred_element_type=f32)
+    def gather(offset, count, place, bank, fade):
+        size = place.stop - place.start
+        new = jnp.dot(vt[:, offset:offset + count], pb[bank, :count, :size], preferred_element_type=f32)
         if fade is not None:
-            new = acc[:, place] * jnp.broadcast_to(fade[:1], (ONES + head_dim, tall)) + new
+            new = acc[:, place] * jnp.broadcast_to(fade[:1], (ONES + head_dim, size)) + new
         acc[:, place] = new
+
+    def block(step):
+        return slice(step * tall, (step + 1) * tall)
 
     def run(tasks, fresh=False):
         score(tasks[0][0], tasks[0][2], 0)
-        fades = []
+        fades, ready = [], []
         for n in range(len(tasks) + 1):
             if n + 1 < len(tasks):
                 score(tasks[n + 1][0], tasks[n + 1][2], (n + 1) % 2)
+            for step, pair in ready:
+                if step:
+                    m_copy(step, pair).start()
+            ready = []
             if n < len(tasks):
                 fades.append(weigh(len(tasks[n][0]) * rows, tasks[n][2], n % 2, fresh))
             if n:
-                slots, offset, step, last = tasks[n - 1]
-                gather(offset, len(slots) * rows, step, (n - 1) % 2, fades[n - 1])
-                if last:
-                    finish(step)
-
-    def m_copy(step):
-        return sp_copy(m_out.at[step], m_all.at[step], load_sem.at[peers + step], m_recv.at[step - 1], first + peer(step))
-
-    def finish(step):
-        for pair in range(heads // 2):
-            halves = []
-            for g in (2 * pair, 2 * pair + 1):
-                piece = acc[:, (step * heads + g) * rows:(step * heads + g + 1) * rows]
-                halves.append(piece[ONES:] * jnp.concatenate([1.0 / piece[:8]] * (head_dim // 8), axis=0))
-            mixed = jnp.concatenate(halves, axis=0).T.astype(bf)
-            (m_out if step else m_all)[step, :, pair * LANES:(pair + 1) * LANES] = mixed
-        if step:
-            m_copy(step).start()
+                slots, offset, place, ready = tasks[n - 1]
+                gather(offset, len(slots) * rows, place, (n - 1) % 2, fades[n - 1])
+                for step, pair in ready:
+                    finish(step, pair)
+        for step, pair in ready:
+            if step:
+                m_copy(step, pair).start()
+
+    def m_copy(step, pair):
+        at = (step - 1) * pairs + pair
+        return sp_copy(m_out.at[step, pair], m_all.at[step, pair], load_sem.at[1 + at], m_recv.at[at], first + peer(step))
+
+    def finish(step, pair):
+        halves = []
+        for g in (2 * pair, 2 * pair + 1):
+            piece = acc[:, (step * heads + g) * rows:(step * heads + g + 1) * rows]
+            halves.append(piece[ONES:] * jnp.concatenate([1.0 / piece[:8]] * (head_dim // 8), axis=0))
+        (m_out if step else m_all)[step, pair] = jnp.concatenate(halves, axis=0).T.astype(bf)
 
     def slots_of(i):
         base, _, needed = onward(i)
@@ -398,7 +409,7 @@
     own = [sp if step == 0 else first + peer(step) for step in near_first]
     spread(0, q_out[0])
     prepare(own, 0)
-    run([(own, 0, 0, False)], fresh=True)
+    run([(own, 0, block(0), ())], fresh=True)
     if groups > 2 and members > 1:
         relay(2, near_first[1:])
     if groups > 3 and members > 1:
@@ -407,7 +418,7 @@
         sp_copy(q_out.at[step], q_all.at[step], load_sem.at[peers + step], q_recv.at[step - 1], first + peer(step)).wait_recv()
         spread(step, q_all[step])
     if members > 1:
-        run([(own, 0, step, False) for step in near_first[1:]], fresh=True)
+        run([(own, 0, block(step), ()) for step in near_first[1:]], fresh=True)
 
     deferred = groups == 4 and members > 1
     spare = 2 * keys
@@ -416,7 +427,7 @@
         slots, needed = slots_of(i)
         fetch(slots, needed)
         prepare(slots, spare)
-        run([(slots, spare, step, False) for step in near_first[1 if deferred else 0:]])
+        run([(slots, spare, block(step), ()) for step in near_first[1 if deferred else 0:]])
         if groups > 4:
             @pl.when(i + 3 < groups)
             def _():
@@ -435,33 +446,48 @@
             fetch(slots, needed)
             prepare(slots, len(last_slots) * rows)
             last_slots += slots
-        tasks = [(last_slots, 0, step, True) for step in far_first]
+        every = tuple(range(pairs))
+        tasks = []
+        for step in far_first[:-1]:
+            if HALVES:
+                tasks += [(last_slots, 0, slice(step * tall + pair * half, step * tall + (pair + 1) * half), ((step, pair),))
+                          for pair in every]
+            else:
+                tasks.append((last_slots, 0, block(step), tuple((step, pair) for pair in every)))
         if deferred:
-            tasks.insert(-1, (slots_of(1)[0], spare, 0, False))
+            tasks.append((slots_of(1)[0], spare, block(0), ()))
+        tasks.append((last_slots, 0, block(0), tuple((0, pair) for pair in every)))
         for step in near_first[1:]:
+            kv_copy(step).wait_send()
             q_copy(step).wait_send()
         run(tasks)
     else:
         for step in near_first[1:]:
+            kv_copy(step).wait_send()
             q_copy(step).wait_send()
         for step in far_first:
-            finish(step)
+            for pair in range(pairs):
+                finish(step, pair)
+                if step:
+                    m_copy(step, pair).start()
 
     loads[small + 5].wait()
     cut_out = wo.shape[1] // O_CUTS
 
     def o_copy(step, j):
         cols = pl.ds(j * cut_out, cut_out)
-        return tp_copy(o_out.at[step, :, cols], o_in.at[step, :, cols], load_sem.at[1 + 2 * peers + (step - 1) * O_CUTS + j], o_recv.at[step - 1, j],
+        return tp_copy(o_out.at[step, :, cols], o_in.at[step, :, cols], load_sem.at[1 + peers * max(2, width // LANES) + (step - 1) * O_CUTS + j], o_recv.at[step - 1, j],
                        (tp + step) % n_tp)
 
     def mixed_share(step, j):
         share = pl.ds(pl.multiple_of(peer(step) * width, width), width)
-        return jnp.dot(m_all[step], wo[share, j * cut_out:(j + 1) * cut_out], preferred_element_type=f32)
+        mixed = jnp.concatenate([m_all[step, pair] for pair in range(pairs)], axis=1)
+        return jnp.dot(mixed, wo[share, j * cut_out:(j + 1) * cut_out], preferred_element_type=f32)
 
     for step in (0, *far_first[:-1]):
         if step:
-            sp_copy(m_out.at[step], m_all.at[step], load_sem.at[peers + step], m_recv.at[step - 1], first + peer(step)).wait_recv()
+            for pair in range(pairs):
+                m_copy(step, pair).wait_recv()
         term = mixed_share(step, 0)
         for j in range(O_CUTS):
             cols = slice(j * cut_out, (j + 1) * cut_out)
@@ -490,8 +516,8 @@
     both_ways(kv_out.at[member], sp, 0, wait_send)
     late_ways(wait_send)
     for step in range(1, members):
-        kv_copy(step).wait_send()
-        m_copy(step).wait_send()
+        for pair in range(pairs):
+            m_copy(step, pair).wait_send()
         both_ways(kv_all.at[first + peer(step)], first + peer(step), step, wait_send)
         if step in crossing:
             straight(step, wait_send)
@@ -556,16 +582,16 @@
                 pltpu.VMEM((2, 2 * members * rows, heads * rows), bf),
                 pltpu.VMEM((ONES + head_dim, members * heads * rows), f32),
                 pltpu.VMEM((8, members * heads * rows), f32),
-                pltpu.VMEM((members, rows, width), bf),
-                pltpu.VMEM((members, rows, width), bf),
+                pltpu.VMEM((members, width // LANES, rows, LANES), bf),
+                pltpu.VMEM((members, width // LANES, rows, LANES), bf),
                 pltpu.VMEM((rows, out_cols), f32),
                 pltpu.VMEM((n_tp, own_rows, out_cols), bf),
                 pltpu.VMEM((n_tp, own_rows, out_cols), bf),
-                dma((max(7 + len(wkv), 1 + 2 * peers + (n_tp - 1) * O_CUTS),)),
+                dma((max(7 + len(wkv), 1 + peers * max(2, width // LANES) + (n_tp - 1) * O_CUTS),)),
                 dma((n_tp - 1, X_CUTS)), dma((n_tp - 1, X_CUTS)),
                 dma((n_sp,)), dma((3 if groups <= 4 else 4, members)),
                 dma((2 if groups <= 4 else groups, members)),
-                dma((peers,)), dma((peers,)),
+                dma((peers,)), dma((peers * (width // LANES),)),
                 dma((n_tp - 1, O_CUTS)),
             ],
             compiler_params=pltpu.CompilerParams(

time: 28 us -> 27.7 us (0.989)
  Pallas kernels: 27.1 us -> 26.8 us
    pallas_call x1, Pallas kernels: 27.1 us -> 26.8 us  [body(): call(tokens_in, w_query, wkv, w_out, jnp.asarray(row_table), jnp.asarray(...]
where the time goes in v3:
time: 27.7 us; the launch traced here: 27.5 us
  Pallas kernels  26.8 us (97%)
  local copies, waits for them, and re-layouts  0.71 us (3%)
    pallas_call x1, Pallas kernels, body(): call(tokens_in, w_query, wkv, w_out, jnp.asarray(row_table), jnp.asarray(...  26.8 us
    unnamed x1, local copies, waits for them, and re-layouts  0.71 us

profile of v3, /device:TPU:0, one launch (start us, length us, event | category | flops | bytes accessed | tf_op | source)
XLA Modules:
  0.0 27.5 jit_solution(4827303388887616144)
XLA Ops:
  0.0 26.8 %shard_map.91 = bf16[64,2048]{1,0:T(8,128)(2,1)S(1)} custom-call(bf16[64,2048]{1,0:T(8,128)(2,1)} %tok_hbm.1, bf16[2048,1024]{1,0:T(8,128)(2,1)} %wq_hbm.1, bf16[2048,256]{1,0:T(8,128)(2,1)} %wkv_hbms_0_.1, bf16[2048,256]{1,0:T(8,128)(2,1)} %wkv_hbms_1_.1, bf16[1024,2048]{1,0:T(8,128)(2,1)} %wo_hbm.1, f32[32,256]{1,0:T(8,128)} %constant.4.clone.row_hbm, ...), custom_call_target="tpu_custom_call" | custom-call | tf_op jit(solution)/shard_map/pallas_call | solution.py:600
  26.8 0.7 %copy.11 = bf16[64,2048]{1,0:T(8,128)(2,1)} copy(bf16[64,2048]{1,0:T(8,128)(2,1)S(1)} %shard_map.91) | data formatting | bytes 524288

commit v4 on v3

--- a/solution.py
+++ b/solution.py
@@ -12,7 +12,7 @@
 LANES = 128
 ONES = 16
 X_CUTS = 1
-O_CUTS = 2
+O_CUTS = 1
 STRAIGHT = (1, 2)
 HALVES = False
 LATE_BESIDE = False

time: 27.7 us -> 27.7 us (level)
  no operation moved by 1% of the time
where the time goes in v4:
time: 27.7 us; the launch traced here: 27.5 us
  Pallas kernels  26.8 us (97%)
  local copies, waits for them, and re-layouts  0.71 us (3%)
    pallas_call x1, Pallas kernels, body(): call(tokens_in, w_query, wkv, w_out, jnp.asarray(row_table), jnp.asarray(...  26.8 us
    unnamed x1, local copies, waits for them, and re-layouts  0.71 us

profile of v4, /device:TPU:0, one launch (start us, length us, event | category | flops | bytes accessed | tf_op | source)
XLA Modules:
  0.0 27.5 jit_solution(9960898956618850887)
XLA Ops:
  0.0 26.8 %shard_map.91 = bf16[64,2048]{1,0:T(8,128)(2,1)S(1)} custom-call(bf16[64,2048]{1,0:T(8,128)(2,1)} %tok_hbm.1, bf16[2048,1024]{1,0:T(8,128)(2,1)} %wq_hbm.1, bf16[2048,256]{1,0:T(8,128)(2,1)} %wkv_hbms_0_.1, bf16[2048,256]{1,0:T(8,128)(2,1)} %wkv_hbms_1_.1, bf16[1024,2048]{1,0:T(8,128)(2,1)} %wo_hbm.1, f32[32,256]{1,0:T(8,128)} %constant.4.clone.row_hbm, ...), custom_call_target="tpu_custom_call" | custom-call | tf_op jit(solution)/shard_map/pallas_call | solution.py:600
  26.8 0.7 %copy.11 = bf16[64,2048]{1,0:T(8,128)(2,1)} copy(bf16[64,2048]{1,0:T(8,128)(2,1)S(1)} %shard_map.91) | data formatting | bytes 524288
